TPU v7x, 1024 devices: a whole 4x8x16 slice. The times are simulated.
1024 devices in a mesh: fs: 128 (over z, y), tp: 8 (over x, core).
Axes of the slice: x: 4, y: 8, z: 16, core: 2. Of those that a mesh axis runs over, the one named last changes fastest.
Arguments:
- hidden_in: bfloat16 [1024, 4096], P(None, 'tp'), may hold values from -6 to 6
- up_act: bfloat16 [1024, 12288], P('tp', 'fs'), may hold values from -6 to 6
- up_val: bfloat16 [1024, 12288], P('tp', 'fs'), may hold values from -6 to 6
- cotangent: bfloat16 [1024, 4096], P('tp'), may hold values from -6 to 6
- w_act: bfloat16 [4096, 12288], P('tp', 'fs'), may hold values from -0.09375 to 0.09375
- w_val: bfloat16 [4096, 12288], P('tp', 'fs'), may hold values from -0.09375 to 0.09375
- w_down: bfloat16 [12288, 4096], P('fs', 'tp'), may hold values from -0.0546875 to 0.0546875
- conv_act: bfloat16 [3, 12288], P(None, 'fs'), may hold values from -3 to 3
- conv_val: bfloat16 [3, 12288], P(None, 'fs'), may hold values from -3 to 3
- bias_act: bfloat16 [12288], P('fs'), may hold values from -3 to 3
- bias_val: bfloat16 [12288], P('fs'), may hold values from -3 to 3
Outputs:
- grad_input: bfloat16 [1024, 4096], P(('tp', 'fs'))
- grad_w_act: float32 [4096, 12288], P('tp', 'fs')
- grad_w_val: float32 [4096, 12288], P('tp', 'fs')
- grad_w_down: float32 [12288, 4096], P('fs', 'tp')
- grad_conv_act: float32 [3, 12288], P(None, 'fs')
- grad_conv_val: float32 [3, 12288], P(None, 'fs')
- grad_bias_act: float32 [12288], P('fs')
- grad_bias_val: float32 [12288], P('fs')
- rows_act: float32 [4096], P('tp')
- rows_val: float32 [4096], P('tp')
- rows_down: float32 [12288], P('fs')
- conv_rows: float32 [2, 3], replicated
All inputs are finite; a program needn't handle non-finite values.
Results may differ from a plain program's by a relative error of at most 0.0057.
Values may be sent and summed in bfloat16 or wider, within the bound.
A program may use at most 32 MiB of HBM per device.

v0:
```python
import jax
import jax.numpy as jnp
from jax import lax
from jax.sharding import Mesh
from jax.sharding import PartitionSpec as P

FS = ("fs_0", "fs_1")
TP = ("tp_0", "tp_1")
TP_FS = ("tp_0", "tp_1", "fs_0", "fs_1")


def rows_first(arrays, axis, dims):
    turned = [jnp.moveaxis(a, dim, 0) for a, dim in zip(arrays, dims)]
    widths = [t[0].size for t in turned]
    both = jnp.concatenate([t.reshape(-1, w) for t, w in zip(turned, widths)], axis=1)
    result = lax.all_gather(both, axis, axis=0, tiled=True)
    parts = jnp.split(result, [sum(widths[:k]) for k in range(1, len(widths))], axis=1)
    return tuple(
        (
            jnp.moveaxis(b.reshape(-1, *t.shape[1:]), 0, dim)
            for b, t, dim in zip(parts, turned, dims)
        )
    )


def passed_along(value, axis, by):
    length = lax.axis_size(axis)
    pairs = [(i, i + by) for i in range(length) if 0 <= i + by < length]
    return lax.ppermute(value, axis, pairs)


def side_by_side(arrays, axis, dim, along):
    ends, at = ([], 0)
    for a in arrays[:-1]:
        at += a.shape[along]
        ends.append(at)
    both = jnp.concatenate(arrays, axis=along)
    return tuple(jnp.split(lax.all_gather(both, axis, axis=dim, tiled=True), ends, axis=along))


def in_blocks(value, dim, length):
    before, after = (value.shape[:dim], value.shape[dim + 1 :])
    return jnp.moveaxis(value.reshape(*before, length, -1, *after), dim, 0)


def laid_out(parts, dim):
    parts = jnp.moveaxis(parts, 0, dim)
    dims = parts.shape
    return parts.reshape(*dims[:dim], dims[dim] * dims[dim + 1], *dims[dim + 2 :])


def turned_blocks(parts, axes, order):
    inside = parts.shape[1:]
    result = parts.reshape(*(lax.axis_size(a) for a in axes), *inside)
    for k in order:
        result = lax.all_to_all(result, axes[k], k, k, tiled=True)
    return result.reshape(-1, *inside)


def exchange_by_axis(value, axes, order, split_dim, concat_dim):
    parts = in_blocks(value, split_dim, lax.axis_size(axes))
    return laid_out(turned_blocks(parts, axes, order), concat_dim)


def sum_by_axis(total, axes):
    for axis in axes:
        total = lax.psum_scatter(total, axis, scatter_dimension=0, tiled=True)
    return total


def copy_for_each(value, axis):
    copies = jnp.broadcast_to(value, (lax.axis_size(axis), *value.shape))
    return lax.all_to_all(copies, axis, split_axis=0, concat_axis=0, tiled=True)


def taken_together(value, axis):
    everything = copy_for_each(value, axis)
    return jnp.sum(everything, axis=0)


def together(arrays, axis):
    ends = [0]
    for a in arrays:
        ends.append(ends[-1] + a.size)
    total = taken_together(jnp.concatenate([a.ravel() for a in arrays]), axis)
    return tuple((total[b:e].reshape(a.shape) for a, b, e in zip(arrays, ends, ends[1:])))


def one_axis_at_a_time(value, axes):
    for axis in axes:
        value = lax.psum(value, axis)
    return value


def contract_last(left, right):
    return lax.dot_general(
        left, right, (((1,), (1,)), ((), ())), preferred_element_type=jnp.float32
    )


def contract_first(left, right):
    return lax.dot_general(
        left, right, (((0,), (0,)), ((), ())), preferred_element_type=jnp.float32
    )


def conv_ahead(extended, taps, bias, length):
    total = jnp.zeros((length, extended.shape[1]), jnp.float32) + bias.astype(jnp.float32)
    for offset in range(taps.shape[0]):
        total = total + taps[offset].astype(jnp.float32) * extended[offset : offset + length]
    return total


def conv_behind(extended, taps, length):
    reach = taps.shape[0] - 1
    total = jnp.zeros((length, extended.shape[1]), jnp.float32)
    for offset in range(taps.shape[0]):
        total = (
            total
            + taps[offset].astype(jnp.float32) * extended[reach - offset : reach - offset + length]
        )
    return total.astype(jnp.bfloat16)


def tap_grads(grad_pre, extended, tap_count):
    length = grad_pre.shape[0]
    rows = [
        jnp.sum(grad_pre * extended[offset : offset + length], axis=0)
        for offset in range(tap_count)
    ]
    return (jnp.stack(rows, 0), jnp.sum(grad_pre, axis=0))


def per_device(
    hidden_in,
    up_act,
    up_val,
    cotangent,
    w_act,
    w_val,
    w_down,
    conv_act,
    conv_val,
    bias_act,
    bias_val,
):
    local_rows = cotangent.shape[0]
    tap_count = conv_act.shape[0]
    reach = tap_count - 1
    act_whole, val_whole, down_whole = rows_first((w_act, w_val, w_down), TP, (0, 0, 1))
    prev_act, prev_val = passed_along(
        (up_act[local_rows - reach :], up_val[local_rows - reach :]), TP, 1
    )
    ext_act = jnp.concatenate([prev_act, up_act], 0).astype(jnp.float32)
    ext_val = jnp.concatenate([prev_val, up_val], 0).astype(jnp.float32)
    pre_act = conv_ahead(ext_act, conv_act, bias_act, local_rows)
    pre_val = conv_ahead(ext_val, conv_val, bias_val, local_rows)
    gelu_act, gelu_back = jax.vjp(jax.nn.gelu, pre_act)
    mixed = (gelu_act * pre_val).astype(jnp.bfloat16)
    grad_mixed = contract_last(cotangent, down_whole).astype(jnp.bfloat16)
    grad_mixed = lax.optimization_barrier(grad_mixed).astype(jnp.float32)
    grad_pre_act = gelu_back(grad_mixed * pre_val)[0]
    grad_pre_val = grad_mixed * gelu_act
    next_act, next_val = passed_along((grad_pre_act[:reach], grad_pre_val[:reach]), TP, -1)
    grad_up_act = conv_behind(jnp.concatenate([grad_pre_act, next_act], 0), conv_act, local_rows)
    grad_up_val = conv_behind(jnp.concatenate([grad_pre_val, next_val], 0), conv_val, local_rows)
    taps_act, sums_act = tap_grads(grad_pre_act, ext_act, tap_count)
    taps_val, sums_val = tap_grads(grad_pre_val, ext_val, tap_count)
    all_up_act, all_up_val, all_mixed = side_by_side((grad_up_act, grad_up_val, mixed), TP, 0, 1)
    cot_columns = exchange_by_axis(cotangent, TP, (1, 0), 1, 0)
    grad_w_act = contract_first(hidden_in, all_up_act)
    grad_w_val = contract_first(hidden_in, all_up_val)
    grad_w_down = contract_first(all_mixed, cot_columns)
    grad_input = sum_by_axis(
        contract_last(grad_up_act, act_whole) + contract_last(grad_up_val, val_whole), FS
    ).astype(jnp.bfloat16)
    down_squares = jnp.sum(grad_w_down * grad_w_down, axis=1)
    taps_act, taps_val, sums_act, sums_val, rows_down = together(
        (taps_act, taps_val, sums_act, sums_val, down_squares), TP
    )
    tap_squares = jnp.stack(
        [jnp.sum(taps_act * taps_act, axis=1), jnp.sum(taps_val * taps_val, axis=1)], 0
    )
    rows_act, rows_val, conv_rows = (
        one_axis_at_a_time(jnp.sum(grad_w_act * grad_w_act, axis=1), FS),
        one_axis_at_a_time(jnp.sum(grad_w_val * grad_w_val, axis=1), FS),
        one_axis_at_a_time(tap_squares, FS),
    )
    return (
        grad_input,
        grad_w_act,
        grad_w_val,
        grad_w_down,
        taps_act,
        taps_val,
        sums_act,
        sums_val,
        rows_act,
        rows_val,
        rows_down,
        conv_rows,
    )


def solution(mesh):
    finer = Mesh(mesh.devices.reshape(16, 8, 4, 2), ("fs_0", "fs_1", "tp_0", "tp_1"))
    return jax.shard_map(
        per_device,
        mesh=finer,
        in_specs=(
            P(None, TP),
            P(TP, FS),
            P(TP, FS),
            P(TP, None),
            P(TP, FS),
            P(TP, FS),
            P(FS, TP),
            P(None, FS),
            P(None, FS),
            P(FS),
            P(FS),
        ),
        out_specs=(
            P(TP_FS, None),
            P(TP, FS),
            P(TP, FS),
            P(FS, TP),
            P(None, FS),
            P(None, FS),
            P(FS),
            P(FS),
            P(TP),
            P(TP),
            P(FS),
            P(),
        ),
        check_vma=False,
    )
```

profile of v0, /device:TPU:6, one launch (start us, length us, event | category | flops | bytes accessed | tf_op | source)
XLA Modules:
  0.0 190.0 jit_solution(10489378691078778796)
XLA Ops:
  7.3 1.8 pad_maximum_fusion
  9.1 0.8 slice.111
  10.0 1.9 %collective-permute-start.1 = (bf16[2,96]{0,1:T(8,128)(2,1)S(1)}, bf16[2,96]{0,1:T(8,128)(2,1)S(1)}, u32[]{:S(2)}, u32[]{:S(2)}) collective-permute-start(bf16[2,96]{0,1:T(8,128)(2,1)S(1)} %slice.111), channel_id=1, source_target_pairs={{0,1},{1,2},{2,3},{3,4},{4,5},{5,6},{6,7},{8,9},{9,10},{10,11},{11... | collective-permute-start | bytes 1160 | tf_op jit(solution)/shard_map/ppermute | solution.py:29
  11.9 0.8 slice.105
  12.7 1.9 %collective-permute-start = (bf16[2,96]{0,1:T(8,128)(2,1)S(1)}, bf16[2,96]{0,1:T(8,128)(2,1)S(1)}, u32[]{:S(2)}, u32[]{:S(2)}) collective-permute-start(bf16[2,96]{0,1:T(8,128)(2,1)S(1)} %slice.105), channel_id=1, source_target_pairs={{0,1},{1,2},{2,3},{3,4},{4,5},{5,6},{6,7},{8,9},{9,10},{10,11},{11... | collective-permute-start | bytes 1160 | tf_op jit(solution)/shard_map/ppermute | solution.py:29
  14.6 0.8 bitcast_convert_fusion.5
  15.4 0.7 convert_element_type.56
  16.1 0.8 maximum_convert_fusion.1
  16.9 0.9 collective-permute-done
  17.8 0.8 maximum_convert_fusion
  18.6 36.1 %all-gather.2.cloned.1.call-done = bf16[4096,288]{0,1:T(8,128)(2,1)} async-done(((bf16[512,288]{0,1:T(8,128)(2,1)}), bf16[4096,288]{0,1:T(8,128)(2,1)}) %all-gather.2.cloned.1.call-update) | async-done | bytes 2359312 | tf_op jit(solution)/shard_map/all_gather | solution.py:16
  54.7 2.1 %fusion = bf16[128,96]{0,1:T(8,128)(2,1)S(1)} fusion(bf16[128,4096]{1,0:T(8,128)(2,1)} %param.14, bf16[4096,288]{0,1:T(8,128)(2,1)} %all-gather.2.cloned.1.call-done), kind=kOutput, calls=%fused_computation.4 | convolution fusion | flops 100675584 | bytes 1859584 | tf_op jit(solution)/shard_map/dot_general | solution.py:96
  57.1 1.9 %collective-permute-start.3 = (f32[2,96]{0,1:T(8,128)S(1)}, f32[2,96]{0,1:T(8,128)S(1)}, u32[]{:S(2)}, u32[]{:S(2)}) collective-permute-start(f32[2,96]{0,1:T(8,128)S(1)} %bitcast.50), channel_id=1, source_target_pairs={{1,0},{2,1},{3,2},{4,3},{5,4},{6,5},{7,6},{9,8},{10,9},{11,10},{12... | collective-permute-start | bytes 2312 | tf_op jit(solution)/shard_map/ppermute | solution.py:29
  59.1 1.7 collective-permute-done.3
  61.1 3.7 %collective-permute-start.2 = (f32[2,96]{0,1:T(8,128)S(1)}, f32[2,96]{0,1:T(8,128)S(1)}, u32[]{:S(2)}, u32[]{:S(2)}) collective-permute-start(f32[2,96]{0,1:T(8,128)S(1)} %bitcast.51), channel_id=1, source_target_pairs={{1,0},{2,1},{3,2},{4,3},{5,4},{6,5},{7,6},{9,8},{10,9},{11,10},{12... | collective-permute-start | bytes 2312 | tf_op jit(solution)/shard_map/ppermute | solution.py:29
  64.8 1.7 collective-permute-done.2
  67.2 1.8 convolution_add_fusion
  69.0 0.7 copy.35
  70.2 4.6 %all_to_all.16 = bf16[4,2,128,512]{3,2,0,1:T(8,128)(2,1)S(1)} all-to-all(bf16[4,2,128,512]{3,2,0,1:T(8,128)(2,1)S(1)} %copy.37), channel_id=1, replica_groups=mesh['fs_0'=16,'fs_1'=8,'tp_0'=4,'tp_1'=2] {'tp_1'}, dimensions={1} | all-to-all | bytes 2097152 | tf_op jit(solution)/shard_map/all_to_all | solution.py:56
  74.8 1.1 copy.38
  75.9 5.6 %all-to-all-start.1 = ((bf16[4,2,128,512]{3,2,1,0:T(8,128)(2,1)}), bf16[4,2,128,512]{3,2,1,0:T(8,128)(2,1)S(1)}, u32[]{:S(2)}, u32[]{:S(2)}) async-start(bf16[4,2,128,512]{3,2,1,0:T(8,128)(2,1)} %copy.38), calls=%async_computation.2 | async-start | bytes 2097152 | tf_op jit(solution)/shard_map/all_to_all | solution.py:56
  81.5 1.3 dynamic-slice
  83.0 19.8 %all_gather.7 = bf16[1024,288]{0,1:T(8,128)(2,1)S(1)} all-gather(bf16[128,288]{0,1:T(8,128)(2,1)S(1)} %pad_maximum_fusion.1), channel_id=1, replica_groups=mesh['fs_0'=16,'fs_1'=8,'tp_0'=4,'tp_1'=2] {'tp_0','tp_1'}, dimensions={0}, use_global_device_ids=true | all-gather | bytes 663552 | tf_op jit(solution)/shard_map/all_gather | solution.py:38
  102.9 1.1 multiply_reduce_fusion.2
  104.6 5.6 %all-to-all-start.2 = ((f32[8,1,864]{2,1,0:T(1,128)}), f32[8,1,864]{2,1,0:T(1,128)S(1)}, u32[]{:S(2)}, u32[]{:S(2)}) async-start(f32[8,1,864]{2,1,0:T(1,128)} %broadcast_in_dim.2), calls=%async_computation.3 | async-start | bytes 57344 | tf_op jit(solution)/shard_map/all_to_all | solution.py:73
  110.2 1.0 multiply_reduce_fusion.1
  111.2 1.0 multiply_reduce_fusion
  112.2 1.4 all-to-all-done.2
  114.1 33.0 %all-reduce.1 = (f32[512]{0:T(512)S(1)}, f32[512]{0:T(512)S(1)}, f32[2,3]{1,0:T(2,128)S(1)}) all-reduce(f32[512]{0:T(512)S(1)} %get-tuple-element.43, f32[512]{0:T(512)S(1)} %get-tuple-element.45, f32[2,3]{1,0:T(2,128)S(1)} %pad_maximum_fusion.6), channel_id=1, replica_groups=mesh['fs_0'=16,'fs_1'=8,'tp_0'=4,'tp_1'=2] {'fs_0'}, use_global_device_ids=true, to_apply=%region_13.0 | all-reduce | flops 1030 | bytes 8240 | tf_op jit(solution)/shard_map/psum | solution.py:91
  147.7 2.4 %reduce-scatter.2.cloned.1.call-done = f32[8,4096]{1,0:T(8,128)} async-done(((f32[128,4096]{1,0:T(8,128)}), f32[8,4096]{1,0:T(8,128)}) %reduce-scatter.2.cloned.1.call-update) | async-done | bytes 131088 | tf_op jit(solution)/shard_map/reduce_scatter | solution.py:67
  150.1 31.8 %all-reduce.4 = (bf16[8,4096]{1,0:T(8,128)(2,1)S(1)}, f32[512]{0:T(512)}, f32[512]{0:T(512)}, f32[2,3]{1,0:T(2,128)}) all-reduce(f32[8,4096]{1,0:T(8,128)} %reduce-scatter.2.cloned.1.call-done, f32[512]{0:T(512)S(1)} %get-tuple-element.20, ...), channel_id=3, replica_groups=mesh['fs_0'=16,'fs_1'=8,'tp_0'=4,'tp_1'=2] {'fs_1'}, use_global_device_ids=true, to_apply=%region_1.0.clone | all-reduce | flops 33798 | bytes 204848
  182.0 1.2 dynamic-slice_convert_fusion
  (43 shorter events, 4.0 us)
Async XLA Ops:
  7.2 103.0 %copy-start = (bf16[1024,512]{1,0:T(8,128)(2,1)S(1)}, bf16[1024,512]{1,0:T(8,128)(2,1)}, u32[]{:S(2)}) copy-start(bf16[1024,512]{1,0:T(8,128)(2,1)} %param.11) | copy-start | bytes 3145732
  7.2 51.9 %copy-start.5 = (bf16[3,96]{1,0:T(4,128)(2,1)S(1)}, bf16[3,96]{1,0:T(4,128)(2,1)}, u32[]{:S(2)}) copy-start(bf16[3,96]{1,0:T(4,128)(2,1)} %param.19) | copy-start | bytes 1732
  7.2 51.9 %copy-start.6 = (bf16[96]{0:T(256)(128)(2,1)S(1)}, bf16[96]{0:T(256)(128)(2,1)}, u32[]{:S(2)}) copy-start(bf16[96]{0:T(256)(128)(2,1)} %param.21) | copy-start | bytes 580
  7.2 47.5 %all-gather.2.cloned.1.call-start = ((), (), s32[]{:S(2)}) async-start(), calls=%async_computation.4 | async-start | bytes 2654208 | tf_op jit(solution)/shard_map/all_gather | solution.py:16
  9.1 141.0 %reduce-scatter.2.cloned.1.call-start = ((), (), s32[]{:S(2)}) async-start(), calls=%async_computation.5 | async-start | bytes 2228224 | tf_op jit(solution)/shard_map/reduce_scatter | solution.py:67
  10.0 6.1 %collective-permute-start.1 = (bf16[2,96]{0,1:T(8,128)(2,1)S(1)}, bf16[2,96]{0,1:T(8,128)(2,1)S(1)}, u32[]{:S(2)}, u32[]{:S(2)}) collective-permute-start(bf16[2,96]{0,1:T(8,128)(2,1)S(1)} %slice.111), channel_id=1, source_target_pairs={{0,1},{1,2},{2,3},{3,4},{4,5},{5,6},{6,7},{8,9},{9,10},{10,11},{11... | collective-permute-start | bytes 1160 | tf_op jit(solution)/shard_map/ppermute | solution.py:29
  12.7 5.1 %collective-permute-start = (bf16[2,96]{0,1:T(8,128)(2,1)S(1)}, bf16[2,96]{0,1:T(8,128)(2,1)S(1)}, u32[]{:S(2)}, u32[]{:S(2)}) collective-permute-start(bf16[2,96]{0,1:T(8,128)(2,1)S(1)} %slice.105), channel_id=1, source_target_pairs={{0,1},{1,2},{2,3},{3,4},{4,5},{5,6},{6,7},{8,9},{9,10},{10,11},{11... | collective-permute-start | bytes 1160 | tf_op jit(solution)/shard_map/ppermute | solution.py:29
  54.7 11.9 %copy-start.2 = (bf16[4096,288]{0,1:T(8,128)(2,1)S(1)}, bf16[4096,288]{0,1:T(8,128)(2,1)}, u32[]{:S(2)}) copy-start(bf16[4096,288]{0,1:T(8,128)(2,1)} %all-gather.2.cloned.1.call-done) | copy-start | bytes 7077892
  57.1 3.7 %collective-permute-start.3 = (f32[2,96]{0,1:T(8,128)S(1)}, f32[2,96]{0,1:T(8,128)S(1)}, u32[]{:S(2)}, u32[]{:S(2)}) collective-permute-start(f32[2,96]{0,1:T(8,128)S(1)} %bitcast.50), channel_id=1, source_target_pairs={{1,0},{2,1},{3,2},{4,3},{5,4},{6,5},{7,6},{9,8},{10,9},{11,10},{12... | collective-permute-start | bytes 2312 | tf_op jit(solution)/shard_map/ppermute | solution.py:29
  61.1 5.4 %collective-permute-start.2 = (f32[2,96]{0,1:T(8,128)S(1)}, f32[2,96]{0,1:T(8,128)S(1)}, u32[]{:S(2)}, u32[]{:S(2)}) collective-permute-start(f32[2,96]{0,1:T(8,128)S(1)} %bitcast.51), channel_id=1, source_target_pairs={{1,0},{2,1},{3,2},{4,3},{5,4},{6,5},{7,6},{9,8},{10,9},{11,10},{12... | collective-permute-start | bytes 2312 | tf_op jit(solution)/shard_map/ppermute | solution.py:29
  67.1 1.9 copy-start.1
  75.9 27.0 %all-to-all-start.1 = ((bf16[4,2,128,512]{3,2,1,0:T(8,128)(2,1)}), bf16[4,2,128,512]{3,2,1,0:T(8,128)(2,1)S(1)}, u32[]{:S(2)}, u32[]{:S(2)}) async-start(bf16[4,2,128,512]{3,2,1,0:T(8,128)(2,1)} %copy.38), calls=%async_computation.2 | async-start | bytes 2097152 | tf_op jit(solution)/shard_map/all_to_all | solution.py:56
  104.6 8.9 %all-to-all-start.2 = ((f32[8,1,864]{2,1,0:T(1,128)}), f32[8,1,864]{2,1,0:T(1,128)S(1)}, u32[]{:S(2)}, u32[]{:S(2)}) async-start(f32[8,1,864]{2,1,0:T(1,128)} %broadcast_in_dim.2), calls=%async_computation.3 | async-start | bytes 57344 | tf_op jit(solution)/shard_map/all_to_all | solution.py:73
  113.8 69.4 %copy-start.3 = (f32[3,96]{1,0:T(4,128)}, f32[3,96]{1,0:T(4,128)S(1)}, u32[]{:S(2)}) copy-start(f32[3,96]{1,0:T(4,128)S(1)} %reshape.69) | copy-start | bytes 3460
  113.8 69.3 %copy-start.4 = (f32[3,96]{1,0:T(4,128)}, f32[3,96]{1,0:T(4,128)S(1)}, u32[]{:S(2)}) copy-start(f32[3,96]{1,0:T(4,128)S(1)} %reshape.68) | copy-start | bytes 3460
Sparse Core Ops, SparseCore 0:
  10.7 43.9 all-gather.1
  69.1 80.9 reduce-scatter.1
where the time goes:
time: 191 us; the launch traced here: 190 us
  blocking collectives  89.3 us (47%)
  waiting for transfers between devices  44.2 us (23%)
  starting transfers between devices  20.7 us (11%)
  between operations  14.3 us (7%)
  local copies, waits for them, and re-layouts  8.12 us (4%)
  matrix products  7.39 us (4%)
  other arithmetic  6.01 us (3%)
    all_gather x1, waiting for transfers between devices, rows_first(): result = lax.all_gather(both, axis, axis=0, tiled=True)  36.1 us
    psum x1, blocking collectives, one_axis_at_a_time(): value = lax.psum(value, axis)  33 us
    unnamed x1, blocking collectives  31.8 us
    all_gather x1, blocking collectives, side_by_side(): lax.all_gather(both, axis, axis=dim, tiled=True)  19.8 us
    ppermute x4, starting transfers between devices, passed_along(): return lax.ppermute(value, axis, pairs)  9.41 us
    all_to_all x1, starting transfers between devices, turned_blocks(): result = lax.all_to_all(result, axes[k], k, k, tiled=True)  5.61 us
    all_to_all x1, starting transfers between devices, copy_for_each(): return lax.all_to_all(copies, axis, split_axis=0, concat_axis=0, tiled=True)  5.56 us
    all_to_all x1, blocking collectives, turned_blocks(): result = lax.all_to_all(result, axes[k], k, k, tiled=True)  4.58 us
  transfers between devices with their start and end apart: 8, of which 6 were waited for; matrix products, arithmetic and copies ran while one was open for 7% of the time, Pallas kernels for 0%

commit v1 on v0

v1 whole, which is shorter than its diff:
```python
import functools

import jax
import jax.numpy as jnp
from jax import lax
from jax.experimental import pallas as pl
from jax.experimental.pallas import tpu as pltpu
from jax.sharding import Mesh
from jax.sharding import PartitionSpec as P

FS = ("fs_0", "fs_1")
TP = ("tp_0", "tp_1")
TP_FS = ("tp_0", "tp_1", "fs_0", "fs_1")
MESH = pl.DeviceIdType.MESH
F32 = jnp.float32
BF16 = jnp.bfloat16
ROOT_2_OVER_PI = 0.7978845608028654
CUBIC = 0.044715


def dot_nn(a, b):
    return lax.dot_general(a, b, (((1,), (0,)), ((), ())), preferred_element_type=F32)


def dot_nt(a, b):
    return lax.dot_general(a, b, (((1,), (1,)), ((), ())), preferred_element_type=F32)


def kernel(
    sizes,
    hid, upa, upv, cot, wa, wv, wd, ca, cv, ba, bv,
    o_gi, o_gwa, o_gwv, o_gwd, o_gca, o_gcv, o_gba, o_gbv, o_ra, o_rv, o_rd, o_cr,
    cotx, hidv, wdall, ea, ev, hpa, hpv, hna, hnv, ga, gv,
    agb, tapb, cotc, lch, wt, ysend, yrecv, acc, zsend, zrecv,
    fsend, frecv, rsend, ryrecv, rzrecv, rfin, drecv,
    lsem, hs, hr, as_, ar, afs, afr, gs, gr, gfs, gfr, ts, tr, cs, cr,
    ys, yr, zs, zr, fs_, fr, r1s, r1r, r2s, r2r, r3s, r3r, ds_, dr,
):
    nz, ny, nx, nc = sizes
    z, y = lax.axis_index("fs_0"), lax.axis_index("fs_1")
    x, c = lax.axis_index("tp_0"), lax.axis_index("tp_1")
    j = x * 2 + c
    rows, hidden = upa.shape
    width = wd.shape[1]
    n = nx * nc
    pend = []

    def send(src, dst, ssem, rsem, device):
        copy = pltpu.make_async_remote_copy(
            src_ref=src, dst_ref=dst, send_sem=ssem, recv_sem=rsem,
            device_id=device, device_id_type=MESH,
        )
        copy.start()
        pend.append(copy)
        return copy

    cot_in = pltpu.make_async_copy(cot, cotx.at[pl.ds(0, rows)], lsem.at[0])
    cot_in.start()
    hid_in = pltpu.make_async_copy(hid, hidv, lsem.at[1])
    hid_in.start()

    barrier = pltpu.get_barrier_semaphore()

    def tp_device(k):
        other = lax.rem(j + k, n)
        return {"tp_0": other // nc, "tp_1": lax.rem(other, nc)}

    for k in range(1, n):
        pl.semaphore_signal(barrier, inc=1, device_id=tp_device(k), device_id_type=MESH)
    for k in range(1, ny):
        pl.semaphore_signal(barrier, inc=1, device_id={"fs_1": lax.rem(y + k, ny)}, device_id_type=MESH)
    for k in range(1, nz):
        pl.semaphore_signal(barrier, inc=1, device_id={"fs_0": lax.rem(z + k, nz)}, device_id_type=MESH)
    pl.semaphore_wait(barrier, n - 1 + ny - 1 + nz - 1)

    partner = {"tp_1": 1 - c}

    def chip(dx):
        return {"tp_0": lax.rem(x + dx, nx)}

    def slot_of(dx, core):
        return lax.rem(x + nx - dx, nx) * 2 + core

    near = (1, 3, 2)
    a_copy = {}
    for dx in near:
        a_copy[dx] = send(wd, wdall.at[j], as_.at[dx], ar.at[dx], chip(dx))
    a_copy[0] = send(wd, wdall.at[j], as_.at[0], ar.at[0], partner)
    up_dev, down_dev = tp_device(1), tp_device(n - 1)
    h_copy = [
        send(cot.at[pl.ds(0, 8)], cotx.at[pl.ds(rows, 8)], hs.at[0], hr.at[0], down_dev),
        send(upa.at[pl.ds(0, 8)], hna, hs.at[1], hr.at[1], down_dev),
        send(upv.at[pl.ds(0, 8)], hnv, hs.at[2], hr.at[2], down_dev),
        send(upa.at[pl.ds(rows - 8, 8)], hpa, hs.at[3], hr.at[3], up_dev),
        send(upv.at[pl.ds(rows - 8, 8)], hpv, hs.at[4], hr.at[4], up_dev),
    ]

    eye = (
        lax.broadcasted_iota(jnp.int32, (hidden, hidden), 0)
        == lax.broadcasted_iota(jnp.int32, (hidden, hidden), 1)
    ).astype(F32).astype(BF16)
    wt[pl.ds(0, hidden), :] = dot_nt(eye, wa[...]).astype(BF16)
    wt[pl.ds(hidden, hidden), :] = dot_nt(eye, wv[...]).astype(BF16)
    out_row = lax.broadcasted_iota(jnp.int32, (rows, rows), 0)
    in_row = lax.broadcasted_iota(jnp.int32, (rows, rows), 1)
    order = (in_row == lax.rem(out_row, nz) * ny + out_row // nz).astype(F32).astype(BF16)

    for copy in h_copy:
        copy.wait_recv()
    first = (j > 0).astype(F32)
    last = (j < n - 1).astype(F32)
    taps_a, taps_v = ca[...].astype(F32), cv[...].astype(F32)
    ext = 8 + rows + 8
    for e, hp, up, hn in ((ea, hpa, upa, hna), (ev, hpv, upv, hnv)):
        e[pl.ds(0, 8), :] = hp[...].astype(F32) * first
        e[pl.ds(8, rows), :] = up[...].astype(F32)
        e[pl.ds(8 + rows, 8), :] = hn[...].astype(F32)
    full = rows + 8

    def ahead(e, taps, bias):
        total = bias[...].astype(F32).reshape(1, hidden) + taps[0:1] * e[pl.ds(6, full), :]
        total = total + taps[1:2] * e[pl.ds(7, full), :]
        return total + taps[2:3] * e[pl.ds(8, full), :]

    pre_a = ahead(ea, taps_a, ba)
    pre_v = ahead(ev, taps_v, bv)
    square = pre_a * pre_a
    th = jnp.tanh(ROOT_2_OVER_PI * (pre_a + CUBIC * pre_a * square))
    half = 0.5 * (1.0 + th)
    gelu = pre_a * half
    slope = half + 0.5 * pre_a * (1.0 - th * th) * (ROOT_2_OVER_PI * (1.0 + 3.0 * CUBIC * square))
    ga[...] = pre_v * slope
    gv[...] = gelu
    mixed = (gelu * pre_v)[0:rows]
    agb[j, pl.ds(2 * hidden, hidden), :] = mixed.T.astype(BF16)

    cot_in.wait()

    def part(slot, block):
        return dot_nt(cotx[:, pl.ds(pl.multiple_of(slot * width, width), width)], block)

    gm = part(j, wd[...])
    a_copy[0].wait_recv()
    gm = gm + part(x * 2 + 1 - c, wdall[x * 2 + 1 - c])
    f_copy = {}
    for dx in near:
        a_copy[dx].wait_recv()
        s = slot_of(dx, c)
        f_copy[dx] = send(wdall.at[s], wdall.at[s], afs.at[dx], afr.at[dx], partner)
        gm = gm + part(s, wdall[s])
    for dx in near:
        f_copy[dx].wait_recv()
        s = slot_of(dx, 1 - c)
        gm = gm + part(s, wdall[s])
    gm = gm.astype(BF16).astype(F32)
    row = lax.broadcasted_iota(jnp.int32, (full, hidden), 0)
    gm = jnp.where(row < rows, gm, gm * last)
    ga[...] = gm * ga[...]
    gv[...] = gm * gv[...]

    def behind(g, taps):
        total = taps[0:1] * g[pl.ds(2, rows), :] + taps[1:2] * g[pl.ds(1, rows), :]
        return total + taps[2:3] * g[pl.ds(0, rows), :]

    agb[j, pl.ds(0, hidden), :] = behind(ga, taps_a).T.astype(BF16)
    agb[j, pl.ds(hidden, hidden), :] = behind(gv, taps_v).T.astype(BF16)
    g_copy = {}
    for dx in near:
        g_copy[dx] = send(agb.at[j], agb.at[j], gs.at[dx], gr.at[dx], chip(dx))
    g_copy[0] = send(agb.at[j], agb.at[j], gs.at[0], gr.at[0], partner)

    at_row = 0
    tapb[j] = jnp.zeros((8, 128), F32)
    for g, e in ((ga, ea), (gv, ev)):
        grad = g[pl.ds(0, rows), :]
        for k in range(3):
            tapb[j, pl.ds(at_row, 1), pl.ds(0, hidden)] = jnp.sum(
                grad * e[pl.ds(6 + k, rows), :], axis=0, keepdims=True
            )
            at_row += 1
        tapb[j, pl.ds(at_row, 1), pl.ds(0, hidden)] = jnp.sum(grad, axis=0, keepdims=True)
        at_row += 1
    t_copy = [
        send(tapb.at[j], tapb.at[j], ts.at[k], tr.at[k], tp_device(k)) for k in range(1, n)
    ]

    def arrange(s):
        ordered = dot_nt(order, agb[s, pl.ds(0, 2 * hidden), :]).astype(BF16)
        for k in range(ny):
            lch[k, pl.ds(pl.multiple_of(s * nz, nz), nz), :] = ordered[k * nz : (k + 1) * nz]

    arrange(j)
    g_copy[0].wait_recv()
    arrange(x * 2 + 1 - c)
    gf_copy = {}
    for dx in near:
        g_copy[dx].wait_recv()
        s = slot_of(dx, c)
        gf_copy[dx] = send(agb.at[s], agb.at[s], gfs.at[dx], gfr.at[dx], partner)
        arrange(s)
    for dx in near:
        gf_copy[dx].wait_recv()
        arrange(slot_of(dx, 1 - c))

    c_copy = []
    for k in range(1, n):
        other = lax.rem(j + k, n)
        c_copy.append(
            send(
                cotx.at[pl.ds(0, rows), pl.ds(pl.multiple_of(other * width, width), width)],
                cotc.at[j], cs.at[k], cr.at[k], tp_device(k),
            )
        )

    wt_all = wt[...]
    wide = width // 2

    def mine(k):
        return dot_nn(lch[lax.rem(y + k + ny, ny)], wt_all)

    def pass_on(i, value, step):
        ysend[i] = value.astype(BF16)
        return send(
            ysend.at[i], yrecv.at[i], ys.at[i], yr.at[i], {"fs_1": lax.rem(y + step + ny, ny)}
        )

    ring = {}

    def arrived(i):
        ring[i].wait_recv()
        return yrecv[i].astype(F32)

    t = mine(4)
    ring[0] = pass_on(0, t[:, :wide], 1)
    ring[7] = pass_on(7, t[:, wide:], -1)
    tp, tm = mine(3), mine(-3)
    ring[4] = pass_on(4, tp[:, wide:], 1)
    ring[11] = pass_on(11, tm[:, :wide], -1)

    hid_in.wait()
    gathered = jnp.concatenate([agb[s, pl.ds(0, 2 * hidden), :] for s in range(n)], axis=1)
    gwt = dot_nn(gathered, hidv[...])
    ring[1] = pass_on(1, arrived(0) + tp[:, :wide], 1)
    ring[8] = pass_on(8, arrived(7) + tm[:, wide:], -1)
    o_gwa[...] = gwt[0:hidden].T
    o_gwv[...] = gwt[hidden:].T
    squares = gwt * gwt
    row_a = jnp.sum(squares[0:hidden], axis=0, keepdims=True)
    row_v = jnp.sum(squares[hidden:], axis=0, keepdims=True)
    tp, tm = mine(2), mine(-2)
    ring[5] = pass_on(5, arrived(4) + tp[:, wide:], 1)
    ring[12] = pass_on(12, arrived(11) + tm[:, :wide], -1)
    for copy in t_copy:
        copy.wait_recv()
    taps = tapb[0]
    for s in range(1, n):
        taps = taps + tapb[s]
    taps = taps[:, 0:hidden]
    o_gca[...] = taps[0:3]
    o_gba[...] = taps[3:4]
    o_gcv[...] = taps[4:7]
    o_gbv[...] = taps[7:8]
    sums = jnp.sum(taps * taps, axis=1, keepdims=True)
    spot = lax.broadcasted_iota(jnp.int32, (8, 128), 0) == lax.broadcasted_iota(
        jnp.int32, (8, 128), 1
    )
    conv_row = jnp.sum(jnp.where(spot, sums, 0.0), axis=0, keepdims=True)
    for k in range(ny):
        source = row_a if k < ny // 2 else row_v
        lane = (k % (ny // 2)) * 128
        rsend[k, pl.ds(0, 1), :] = source[:, lane : lane + 128]
        rsend[k, pl.ds(1, 1), :] = conv_row
    r1_copy = []
    for k in range(1, ny):
        other = lax.rem(y + k, ny)
        r1_copy.append(
            send(rsend.at[other], ryrecv.at[y], r1s.at[k], r1r.at[k], {"fs_1": other})
        )
    ryrecv[y] = rsend[y]
    ring[2] = pass_on(2, arrived(1) + tp[:, :wide], 1)
    ring[9] = pass_on(9, arrived(8) + tm[:, wide:], -1)
    tp, tm = mine(1), mine(-1)
    ring[6] = pass_on(6, arrived(5) + tp[:, wide:], 1)
    ring[13] = pass_on(13, arrived(12) + tm[:, :wide], -1)
    ring[3] = pass_on(3, arrived(2) + tp[:, :wide], 1)
    ring[10] = pass_on(10, arrived(9) + tm[:, wide:], -1)
    for copy in r1_copy:
        copy.wait_recv()
    piece = ryrecv[0]
    for s in range(1, ny):
        piece = piece + ryrecv[s]
    rzrecv[z] = piece
    r2_copy = [
        send(rzrecv.at[z], rzrecv.at[z], r2s.at[k], r2r.at[k], {"fs_0": lax.rem(z + k, nz)})
        for k in range(1, nz)
    ]
    t = mine(0)
    lanes_b = t[:, wide:] + (arrived(6) + arrived(10))
    lanes_a = t[:, :wide] + (arrived(13) + arrived(3))
    tiles = width // 128
    for k in range(tiles // 2):
        acc[k] = lanes_a[:, 128 * k : 128 * (k + 1)]
        acc[tiles // 2 + k] = lanes_b[:, 128 * k : 128 * (k + 1)]

    for k in range(nz):
        for i in range(tiles):
            zsend[k, :, pl.ds(128 * i, 128)] = acc[i, pl.ds(k, n, stride=nz), :].astype(BF16)
    z_copy = []
    for k in range(1, nz):
        other = lax.rem(z + k, nz)
        z_copy.append(send(zsend.at[other], zrecv.at[z], zs.at[k], zr.at[k], {"fs_0": other}))
    zrecv[z] = zsend[z]

    for copy in c_copy:
        copy.wait_recv()
    cotc[j] = cotx[pl.ds(0, rows), pl.ds(pl.multiple_of(j * width, width), width)]
    mixed_all = jnp.concatenate([agb[s, pl.ds(2 * hidden, hidden), :] for s in range(n)], axis=1)
    gwd = dot_nn(mixed_all, cotc[...].reshape(n * rows, width))
    o_gwd[...] = gwd
    sq = gwd * gwd
    lanes = sq[:, 0:128]
    for k in range(1, width // 128):
        lanes = lanes + sq[:, 128 * k : 128 * (k + 1)]
    drecv[j] = jnp.zeros((1, 128), F32)
    drecv[j, :, pl.ds(0, hidden)] = jnp.sum(lanes.T, axis=0, keepdims=True)
    d_copy = [
        send(drecv.at[j], drecv.at[j], ds_.at[k], dr.at[k], tp_device(k)) for k in range(1, n)
    ]

    for copy in r2_copy:
        copy.wait_recv()
    piece = rzrecv[0]
    for s in range(1, nz):
        piece = piece + rzrecv[s]
    rfin[y] = piece
    r3_copy = [
        send(rfin.at[y], rfin.at[y], r3s.at[k], r3r.at[k], {"fs_1": lax.rem(y + k, ny)})
        for k in range(1, ny)
    ]
    o_cr[...] = piece[1:2]

    for copy in z_copy:
        copy.wait_recv()
    total = zrecv[0].astype(F32)
    for s in range(1, nz):
        total = total + zrecv[s].astype(F32)
    for s in range(n):
        fsend[s] = total[s : s + 1]
    f2_copy = []
    for k in range(1, n):
        other = lax.rem(j + k, n)
        f2_copy.append(send(fsend.at[other], frecv.at[j], fs_.at[k], fr.at[k], tp_device(k)))
    frecv[j] = fsend[j]

    for copy in d_copy:
        copy.wait_recv()
    down = drecv[0]
    for s in range(1, n):
        down = down + drecv[s]
    o_rd[...] = down
    for copy in r3_copy:
        copy.wait_recv()
    half_n = ny // 2
    for k in range(half_n):
        o_ra[:, pl.ds(128 * k, 128)] = rfin[k, pl.ds(0, 1), :]
        o_rv[:, pl.ds(128 * k, 128)] = rfin[half_n + k, pl.ds(0, 1), :]
    for copy in f2_copy:
        copy.wait_recv()
    for s in range(n):
        o_gi[:, pl.ds(width * s, width)] = frecv[s].astype(BF16)
    for copy in pend:
        copy.wait_send()


def per_device(sizes, hid, upa, upv, cot, wa, wv, wd, ca, cv, ba, bv):
    nz, ny, nx, nc = sizes
    n = nx * nc
    rows, hidden = upa.shape
    width = wd.shape[1]
    tokens = hid.shape[0]
    vm = pl.BlockSpec(memory_space=pltpu.VMEM)
    hbm = pl.BlockSpec(memory_space=pl.ANY)
    dma = pltpu.SemaphoreType.DMA

    def f32(*shape):
        return jax.ShapeDtypeStruct(shape, F32)

    outs = (
        jax.ShapeDtypeStruct((1, n * width), BF16),
        f32(width, hidden), f32(width, hidden), f32(hidden, width),
        f32(3, hidden), f32(3, hidden), f32(1, hidden), f32(1, hidden),
        f32(1, width), f32(1, width), f32(1, 128), f32(1, 128),
    )
    v = pltpu.VMEM
    scratch = [
        v((rows + 8, n * width), BF16), v((tokens, width), BF16), v((n, hidden, width), BF16),
        v((rows + 16, hidden), F32), v((rows + 16, hidden), F32),
        v((8, hidden), BF16), v((8, hidden), BF16), v((8, hidden), BF16), v((8, hidden), BF16),
        v((rows + 8, hidden), F32), v((rows + 8, hidden), F32),
        v((n, 3 * hidden, rows), BF16), v((n, 8, 128), F32), v((n, rows, width), BF16),
        v((ny, rows, 2 * hidden), BF16), v((2 * hidden, width), BF16),
        v((14, rows, width // 2), BF16), v((14, rows, width // 2), BF16),
        v((width // 128, rows, 128), F32), v((nz, n, width), BF16), v((nz, n, width), BF16),
        v((n, 1, width), F32), v((n, 1, width), F32),
        v((ny, 2, 128), F32), v((ny, 2, 128), F32), v((nz, 2, 128), F32), v((ny, 2, 128), F32),
        v((n, 1, 128), F32),
        dma((2,)), dma((5,)), dma((5,)), dma((4,)), dma((4,)), dma((4,)), dma((4,)),
        dma((4,)), dma((4,)), dma((4,)), dma((4,)), dma((n,)), dma((n,)), dma((n,)), dma((n,)),
        dma((14,)), dma((14,)), dma((nz,)), dma((nz,)), dma((n,)), dma((n,)),
        dma((ny,)), dma((ny,)), dma((nz,)), dma((nz,)), dma((ny,)), dma((ny,)),
        dma((n,)), dma((n,)),
    ]
    res = pl.pallas_call(
        functools.partial(kernel, sizes),
        out_shape=outs,
        in_specs=[hbm, vm, vm, hbm, vm, vm, vm, vm, vm, vm, vm],
        out_specs=[vm] * len(outs),
        scratch_shapes=scratch,
        compiler_params=pltpu.CompilerParams(
            collective_id=0, has_side_effects=True, vmem_limit_bytes=48 * 1024 * 1024
        ),
    )(hid, upa, upv, cot, wa, wv, wd, ca, cv, ba, bv)
    gi, gwa, gwv, gwd, gca, gcv, gba, gbv, ra, rv, rd, cr = res
    conv_rows = jnp.stack([cr[0, 0:3], cr[0, 4:7]], 0)
    return (
        gi, gwa, gwv, gwd, gca, gcv, gba[0], gbv[0], ra[0], rv[0], rd[0, :hidden], conv_rows,
    )


def solution(mesh):
    sizes = (16, 8, 4, 2)
    finer = Mesh(mesh.devices.reshape(sizes), FS + TP)
    return jax.shard_map(
        functools.partial(per_device, sizes),
        mesh=finer,
        in_specs=(
            P(None, TP), P(TP, FS), P(TP, FS), P(TP, None), P(TP, FS), P(TP, FS),
            P(FS, TP), P(None, FS), P(None, FS), P(FS), P(FS),
        ),
        out_specs=(
            P(TP_FS, None), P(TP, FS), P(TP, FS), P(FS, TP), P(None, FS), P(None, FS),
            P(FS), P(FS), P(TP), P(TP), P(FS), P(),
        ),
        check_vma=False,
    )
```

time: 191 us -> 84.7 us (0.44)
  the two profiles are of different devices: /device:TPU:6 before, /device:TPU:1 now
where the time goes in v1:
time: 84.7 us; the launch traced here: 84.3 us
  Pallas kernels  70.3 us (83%)
  local copies, waits for them, and re-layouts  12.7 us (15%)
    pallas_call x1, Pallas kernels, per_device(): pl.pallas_call(functools.partial(kernel, sizes), out_shape=outs, in_specs...  70.3 us
    unnamed x32, local copies, waits for them, and re-layouts  12.2 us

profile of v1, /device:TPU:1, one launch (start us, length us, event | category | flops | bytes accessed | tf_op | source)
XLA Modules:
  0.0 84.3 jit_solution(16245472498880491036)
XLA Ops:
  0.6 0.0 copy-start.7
  0.7 0.9 %copy.23.upa = bf16[128,96]{1,0:T(8,128)(2,1)S(1)} copy(bf16[128,96]{0,1:T(8,128)(2,1)} %param.12) | data formatting | bytes 49152 | tf_op args[1]
  1.5 0.9 %copy.24.upv = bf16[128,96]{1,0:T(8,128)(2,1)S(1)} copy(bf16[128,96]{0,1:T(8,128)(2,1)} %param.13) | data formatting | bytes 49152 | tf_op args[2]
  2.4 0.0 copy-done.7
  2.4 0.0 copy-start.8
  2.4 0.1 copy.25.wa
  2.5 0.8 copy-done.8
  3.3 0.0 copy-start.2
  3.3 0.0 copy-start.6
  3.3 0.1 copy.26.wv
  3.4 0.7 copy-done.2
  4.2 0.0 copy-done.3
  4.2 0.0 copy-done.4
  4.2 0.0 copy-done.5
  4.2 0.0 copy-done.6
  4.2 0.0 copy-start
  4.2 1.2 %copy-done = bf16[1024,512]{1,0:T(8,128)(2,1)S(1)} copy-done((bf16[1024,512]{1,0:T(8,128)(2,1)S(1)}, bf16[1024,512]{1,0:T(8,128)(2,1)}, u32[]{:S(2)}) %copy-start) | copy-done | bytes 1048600
  5.4 1.2 %copy-done.1 = bf16[128,4096]{1,0:T(8,128)(2,1)S(1)} copy-done((bf16[128,4096]{1,0:T(8,128)(2,1)S(1)}, bf16[128,4096]{1,0:T(8,128)(2,1)}, u32[]{:S(2)}) %copy-start.1) | copy-done | bytes 1048600
  6.7 70.3 %shard_map.202 = (bf16[1,4096]{1,0:T(2,128)(2,1)S(1)}, f32[512,96]{1,0:T(8,128)S(1)}, f32[512,96]{1,0:T(8,128)S(1)}, f32[96,512]{1,0:T(8,128)S(1)}, f32[3,96]{1,...) custom-call(bf16[1024,512]{1,0:T(8,128)(2,1)S(1)} %copy-done, ...), custom_call_target="tpu_custom_call" | custom-call | tf_op jit(solution)/shard_map/pallas_call | solution.py:413
  76.9 0.5 slice_bitcast_fusion
  77.4 0.1 fusion
  77.5 0.6 pad_maximum_fusion
  78.1 0.8 copy.27
  78.9 0.8 copy.28
  79.7 0.6 copy.37
  80.3 0.7 copy.38
  81.0 0.6 copy.39
  81.5 0.6 copy.40
  82.1 0.5 copy.41
  82.6 0.5 copy.42
  83.1 0.6 copy.43
  83.7 0.6 copy.44
  (4 shorter events, 0.0 us)
Async XLA Ops:
  0.6 1.7 %copy-start.7 = (bf16[512,96]{0,1:T(8,128)(2,1)S(1)}, bf16[512,96]{0,1:T(8,128)(2,1)}, u32[]{:S(2)}) copy-start(bf16[512,96]{0,1:T(8,128)(2,1)} %param.15) | copy-start | bytes 294916
  2.4 0.9 %copy-start.8 = (bf16[512,96]{0,1:T(8,128)(2,1)S(1)}, bf16[512,96]{0,1:T(8,128)(2,1)}, u32[]{:S(2)}) copy-start(bf16[512,96]{0,1:T(8,128)(2,1)} %param.16) | copy-start | bytes 294916
  3.3 0.9 %copy-start.2 = (bf16[96,512]{1,0:T(8,128)(2,1)S(1)}, bf16[96,512]{1,0:T(8,128)(2,1)}, u32[]{:S(2)}) copy-start(bf16[96,512]{1,0:T(8,128)(2,1)} %wd.1) | copy-start | bytes 294916
  3.3 0.9 %copy-start.3 = (bf16[3,96]{1,0:T(4,128)(2,1)S(1)}, bf16[3,96]{1,0:T(4,128)(2,1)}, u32[]{:S(2)}) copy-start(bf16[3,96]{1,0:T(4,128)(2,1)} %ca.1) | copy-start | bytes 1732
  3.3 0.9 %copy-start.4 = (bf16[3,96]{1,0:T(4,128)(2,1)S(1)}, bf16[3,96]{1,0:T(4,128)(2,1)}, u32[]{:S(2)}) copy-start(bf16[3,96]{1,0:T(4,128)(2,1)} %cv.1) | copy-start | bytes 1732
  3.3 0.9 %copy-start.5 = (bf16[96]{0:T(256)(128)(2,1)S(1)}, bf16[96]{0:T(256)(128)(2,1)}, u32[]{:S(2)}) copy-start(bf16[96]{0:T(256)(128)(2,1)} %ba.1) | copy-start | bytes 580
  3.3 0.9 %copy-start.6 = (bf16[96]{0:T(256)(128)(2,1)S(1)}, bf16[96]{0:T(256)(128)(2,1)}, u32[]{:S(2)}) copy-start(bf16[96]{0:T(256)(128)(2,1)} %bv.1) | copy-start | bytes 580
  4.2 1.2 %copy-start = (bf16[1024,512]{1,0:T(8,128)(2,1)S(1)}, bf16[1024,512]{1,0:T(8,128)(2,1)}, u32[]{:S(2)}) copy-start(bf16[1024,512]{1,0:T(8,128)(2,1)} %hid.1) | copy-start | bytes 3145732
  5.4 1.2 %copy-start.1 = (bf16[128,4096]{1,0:T(8,128)(2,1)S(1)}, bf16[128,4096]{1,0:T(8,128)(2,1)}, u32[]{:S(2)}) copy-start(bf16[128,4096]{1,0:T(8,128)(2,1)} %cot.1) | copy-start | bytes 3145732

commit v2 on v1

v2 whole, which is shorter than its diff:
```python
import functools

import jax
import jax.numpy as jnp
from jax import lax
from jax.experimental import pallas as pl
from jax.experimental.pallas import tpu as pltpu
from jax.sharding import Mesh
from jax.sharding import PartitionSpec as P

FS = ("fs_0", "fs_1")
TP = ("tp_0", "tp_1")
TP_FS = ("tp_0", "tp_1", "fs_0", "fs_1")
MESH = pl.DeviceIdType.MESH
F32 = jnp.float32
BF16 = jnp.bfloat16
ROOT_2_OVER_PI = 0.7978845608028654
CUBIC = 0.044715


def dot_nn(a, b):
    return lax.dot_general(a, b, (((1,), (0,)), ((), ())), preferred_element_type=F32)


def dot_nt(a, b):
    return lax.dot_general(a, b, (((1,), (1,)), ((), ())), preferred_element_type=F32)


def kernel(
    sizes,
    hid, upa, upv, cot, wa, wv, wd, ca, cv, ba, bv,
    o_gi, o_gwa, o_gwv, o_gwd, o_tap, o_ra, o_rv, o_rd, o_cr,
    cotx, hidv, wdall, wall, uas, uvs, cas, cvs, bas, bvs, hb, hprev, hnext,
    agb, tapb, cotc, relay, pbuf, ysend, yrecv, acc, zsend, zrecv, row_out,
    rz, ry, drecv,
    lsem, hs, hr, wds_, wdr, was, war, wvs, wvr, gs, gr, ts, tr, cs, cr,
    ys, yr, zs, zr, r1s, r1r, r2s, r2r, ds_, dr,
):
    nz, ny, nx, nc = sizes
    z, y = lax.axis_index("fs_0"), lax.axis_index("fs_1")
    x, c = lax.axis_index("tp_0"), lax.axis_index("tp_1")
    j = x * 2 + c
    hidden, rows = upa.shape
    width = wd.shape[1]
    n = nx * nc
    pend = []

    def send(src, dst, ssem, rsem, device):
        copy = pltpu.make_async_remote_copy(
            src_ref=src, dst_ref=dst, send_sem=ssem, recv_sem=rsem,
            device_id=device, device_id_type=MESH,
        )
        copy.start()
        pend.append(copy)
        return copy

    barrier = pltpu.get_barrier_semaphore()

    def tp_device(k):
        other = lax.rem(j + k, n)
        return {"tp_0": other // nc, "tp_1": lax.rem(other, nc)}

    for k in range(1, nz):
        pl.semaphore_signal(barrier, inc=1, device_id={"fs_0": lax.rem(z + k, nz)}, device_id_type=MESH)
    for k in range(1, ny):
        pl.semaphore_signal(barrier, inc=1, device_id={"fs_1": lax.rem(y + k, ny)}, device_id_type=MESH)
    for k in range(1, n):
        pl.semaphore_signal(barrier, inc=1, device_id=tp_device(k), device_id_type=MESH)

    loads = []
    for i, (src, dst) in enumerate((
        (wd, wdall.at[j]), (upa, uas), (upv, uvs), (ca, cas), (cv, cvs), (ba, bas), (bv, bvs),
        (cot, cotx.at[pl.ds(0, rows)]), (wa, wall.at[j, pl.ds(0, hidden)]),
        (wv, wall.at[j, pl.ds(hidden, hidden)]), (hid, hidv),
    )):
        copy = pltpu.make_async_copy(src, dst, lsem.at[i])
        copy.start()
        loads.append(copy)
    for copy in loads[0:7]:
        copy.wait()

    lane = lax.broadcasted_iota(jnp.int32, (hidden, rows), 1)

    def roll(value, by):
        return pltpu.roll(value, by % rows, 1)

    ua, uv = uas[...].astype(F32), uvs[...].astype(F32)
    heads = jnp.where(lane < 2, ua, roll(uv, 2))
    tails = jnp.where(lane >= rows - 2, ua, roll(uv, -2))
    hb[...] = jnp.where(lane < rows // 2, heads, tails).astype(BF16)

    pl.semaphore_wait(barrier, n - 1 + ny - 1 + nz - 1)

    partner = {"tp_1": 1 - c}

    def chip(dx):
        return {"tp_0": lax.rem(x + dx, nx)}

    def slot_of(dx, core):
        return lax.rem(x + nx - dx, nx) * 2 + core

    slots = (
        j, x * 2 + 1 - c, slot_of(1, c), slot_of(3, c),
        slot_of(1, 1 - c), slot_of(3, 1 - c), slot_of(2, c), slot_of(2, 1 - c),
    )

    class Gather:
        def __init__(self, buf, first, count, ssem, rsem):
            self.buf, self.first, self.count, self.half = buf, first, count, count // 2
            self.ssem, self.rsem, self.copies = ssem, rsem, {}

        def go(self, i, slot, at, size, device):
            view = self.buf.at[slot, pl.ds(self.first + at, size)]
            self.copies[i] = send(view, view, self.ssem.at[i], self.rsem.at[i], device)

        def start(self):
            self.go(1, j, 0, self.count, chip(1))
            self.go(2, j, 0, self.count, chip(3))
            self.go(0, j, 0, self.count, partner)

        def wait(self, *which):
            for i in which:
                self.copies[i].wait_recv()

        def pass_near(self):
            self.wait(1)
            self.go(3, slots[2], 0, self.half, chip(1))
            self.go(5, slots[2], 0, self.count, partner)
            self.wait(2)
            self.go(4, slots[3], self.half, self.half, chip(3))
            self.go(6, slots[3], 0, self.count, partner)

        def pass_far(self):
            self.wait(3)
            self.go(7, slots[6], 0, self.half, partner)
            self.wait(4)
            self.go(8, slots[6], self.half, self.half, partner)

    down_all = Gather(wdall, 0, hidden, wds_, wdr)
    act_all = Gather(wall, 0, hidden, was, war)
    val_all = Gather(wall, hidden, hidden, wvs, wvr)
    grads_all = Gather(agb, 0, 3 * hidden, gs, gr)
    down_all.start()
    up_dev, down_dev = tp_device(1), tp_device(n - 1)
    h_copy = [
        send(cot.at[pl.ds(0, 8)], cotx.at[pl.ds(rows, 8)], hs.at[0], hr.at[0], down_dev),
        send(hb, hnext, hs.at[1], hr.at[1], down_dev),
        send(hb, hprev, hs.at[2], hr.at[2], up_dev),
    ]

    for copy in loads[8:10]:
        copy.wait()
    act_all.start()

    out_row = lax.broadcasted_iota(jnp.int32, (rows, rows), 0)
    in_row = lax.broadcasted_iota(jnp.int32, (rows, rows), 1)
    order = (in_row == lax.rem(out_row, nz) * ny + out_row // nz).astype(F32).astype(BF16)
    table = jnp.concatenate(
        [cas[...].astype(F32), bas[...].astype(F32).reshape(1, hidden),
         cvs[...].astype(F32), bvs[...].astype(F32).reshape(1, hidden)], axis=0,
    ).T
    par_a = [table[:, k : k + 1] for k in range(4)]
    par_v = [table[:, k : k + 1] for k in range(4, 8)]

    for copy in h_copy:
        copy.wait_recv()
    first = (j > 0).astype(F32)
    last = (j < n - 1).astype(F32)
    before = hprev[...].astype(F32) * first
    after = hnext[...].astype(F32)

    def ahead(par, u2, u1, u0):
        return par[3] + par[0] * u2 + par[1] * u1 + par[2] * u0

    def shifted(u, prev):
        u1 = jnp.where(lane < 1, roll(prev, 1), roll(u, 1))
        return jnp.where(lane < 2, roll(prev, 2), roll(u, 2)), u1, u

    def shifted_next(u, following):
        u1 = jnp.where(lane < 1, roll(u, 1), roll(following, 1))
        return [v[:, 0:8] for v in (roll(u, 2), u1, following)]

    ups_a = shifted(ua, before)
    ups_v = shifted(uv, roll(before, 2))
    next_a = shifted_next(ua, after)
    next_v = shifted_next(uv, roll(after, -2))

    def activation(pre_a, pre_v):
        square = pre_a * pre_a
        th = jnp.tanh(ROOT_2_OVER_PI * (pre_a + CUBIC * pre_a * square))
        half = 0.5 * (1.0 + th)
        gelu = pre_a * half
        slope = half + 0.5 * pre_a * (1.0 - th * th) * (ROOT_2_OVER_PI * (1.0 + 3.0 * CUBIC * square))
        return pre_v * slope, gelu, gelu * pre_v

    fac_a, fac_v, mixed = activation(ahead(par_a, *ups_a), ahead(par_v, *ups_v))
    nfac_a, nfac_v, _ = activation(ahead(par_a, *next_a), ahead(par_v, *next_v))
    agb[j, pl.ds(2 * hidden, hidden), :] = mixed.astype(BF16)

    loads[7].wait()

    def part(slot, block):
        return dot_nt(block, cotx[:, pl.ds(pl.multiple_of(slot * width, width), width)])

    gm = part(j, wdall[j])
    down_all.wait(0)
    gm = gm + part(slots[1], wdall[slots[1]])
    down_all.pass_near()
    val_all.start()
    gm = gm + part(slots[2], wdall[slots[2]]) + part(slots[3], wdall[slots[3]])
    down_all.wait(5, 6)
    gm = gm + part(slots[4], wdall[slots[4]]) + part(slots[5], wdall[slots[5]])
    act_all.pass_near()
    down_all.pass_far()
    gm = gm + part(slots[6], wdall[slots[6]])
    down_all.wait(7, 8)
    gm = gm + part(slots[7], wdall[slots[7]])
    gm = gm.astype(BF16).astype(F32)
    gm_next = gm[:, rows:] * last
    gm = gm[:, 0:rows]
    grad_a, grad_v = gm * fac_a, gm * fac_v
    empty = jnp.zeros((hidden, rows - 8), F32)
    after_a = jnp.concatenate([gm_next * nfac_a, empty], axis=1)
    after_v = jnp.concatenate([gm_next * nfac_v, empty], axis=1)

    def behind(par, grad, following):
        g1 = jnp.where(lane < rows - 1, roll(grad, -1), roll(following, -1))
        g2 = jnp.where(lane < rows - 2, roll(grad, -2), roll(following, -2))
        return par[0] * g2 + par[1] * g1 + par[2] * grad

    agb[j, pl.ds(0, hidden), :] = behind(par_a, grad_a, after_a).astype(BF16)
    agb[j, pl.ds(hidden, hidden), :] = behind(par_v, grad_v, after_v).astype(BF16)
    val_all.pass_near()
    grads_all.start()
    left = dot_nt(order, agb[j, pl.ds(0, 2 * hidden), :]).astype(BF16)

    spread = jnp.zeros((hidden, rows), F32)
    at = 0
    for grad, ups in ((grad_a, ups_a), (grad_v, ups_v)):
        for k in range(4):
            terms = grad * ups[k] if k < 3 else grad
            spread = jnp.where(lane == at, jnp.sum(terms, axis=1, keepdims=True), spread)
            at += 1
    tapb[j] = spread.T[0:8]
    t_copy = [
        send(tapb.at[j], tapb.at[j], ts.at[k], tr.at[k], tp_device(k)) for k in range(1, n)
    ]

    def product(a):
        pbuf[a] = dot_nn(left, wall[slots[a]])

    def mine(k, half):
        at = pl.multiple_of(lax.rem(y + k + ny, ny) * nz, nz)
        return pbuf[pl.ds(4 * half, 4), pl.ds(at, nz), :]

    ring = {}

    def pass_on(i, value, step):
        ysend[i] = value.astype(BF16)
        ring[i] = send(
            ysend.at[i], yrecv.at[i], ys.at[i], yr.at[i], {"fs_1": lax.rem(y + step + ny, ny)}
        )

    def arrived(i):
        ring[i].wait_recv()
        return yrecv[i].astype(F32)

    product(0)
    act_all.wait(0)
    val_all.wait(0)
    product(1)
    product(2)
    product(3)
    pass_on(0, mine(4, 0), 1)
    pass_on(11, mine(-3, 0), -1)
    act_all.wait(5, 6)
    val_all.wait(5, 6)
    product(4)
    product(5)
    act_all.pass_far()
    val_all.pass_far()
    product(6)
    act_all.wait(7, 8)
    val_all.wait(7, 8)
    product(7)
    pass_on(7, mine(-4, 1), -1)
    pass_on(4, mine(3, 1), 1)
    grads_all.pass_near()
    pass_on(1, arrived(0) + mine(3, 0), 1)
    pass_on(12, arrived(11) + mine(-2, 0), -1)

    def columns(dx, core):
        at = (lax.rem(x + dx, nx) * 2 + core) * width
        return cotx.at[pl.ds(0, rows), pl.ds(pl.multiple_of(at, width), width)]

    c_copy = [
        send(columns(2, 1 - c), relay, cs.at[6], cr.at[6], {"tp_0": lax.rem(x + 3, nx), "tp_1": 1 - c})
    ]
    for i, (dx, core) in enumerate(((1, c), (3, c), (2, c), (1, 1 - c), (3, 1 - c), (0, 1 - c))):
        c_copy.append(
            send(
                columns(dx, core), cotc.at[j], cs.at[i], cr.at[i],
                {"tp_0": lax.rem(x + dx, nx), "tp_1": core},
            )
        )
    pass_on(8, arrived(7) + mine(-3, 1), -1)
    pass_on(5, arrived(4) + mine(2, 1), 1)
    pass_on(2, arrived(1) + mine(2, 0), 1)
    pass_on(13, arrived(12) + mine(-1, 0), -1)

    grads_all.wait(0, 5, 6)
    grads_all.pass_far()
    grads_all.wait(7, 8)
    loads[10].wait()
    gathered = jnp.concatenate([agb[s, pl.ds(0, 2 * hidden), :] for s in range(n)], axis=1)
    gwt = dot_nn(gathered, hidv[...])
    o_gwa[...] = gwt[0:hidden]
    o_gwv[...] = gwt[hidden:]
    squares = gwt * gwt
    row_a = jnp.sum(squares[0:hidden], axis=0, keepdims=True)
    row_v = jnp.sum(squares[hidden:], axis=0, keepdims=True)
    for copy in t_copy:
        copy.wait_recv()
    taps = tapb[0]
    for s in range(1, n):
        taps = taps + tapb[s]
    o_tap[...] = taps
    sums = jnp.sum(taps * taps, axis=1, keepdims=True)
    spot = lax.broadcasted_iota(jnp.int32, (8, 128), 0) == lax.broadcasted_iota(
        jnp.int32, (8, 128), 1
    )
    tiles = width // 128
    for k in range(tiles):
        rz[z, k] = row_a[:, 128 * k : 128 * (k + 1)]
        rz[z, tiles + k] = row_v[:, 128 * k : 128 * (k + 1)]
    rz[z, 2 * tiles] = jnp.sum(jnp.where(spot, sums, 0.0), axis=0, keepdims=True)
    r1_copy = [
        send(rz.at[z], rz.at[z], r1s.at[k], r1r.at[k], {"fs_0": lax.rem(z + k, nz)})
        for k in range(1, nz)
    ]

    pass_on(9, arrived(8) + mine(-2, 1), -1)
    pass_on(6, arrived(5) + mine(1, 1), 1)
    pass_on(3, arrived(2) + mine(1, 0), 1)
    c_copy[0].wait_recv()
    c_copy.append(send(relay, cotc.at[slot_of(3, 1 - c)], cs.at[7], cr.at[7], chip(3)))
    pass_on(10, arrived(9) + mine(-1, 1), -1)
    for half, (i, k) in enumerate(((13, 3), (6, 10))):
        total = mine(0, half) + (arrived(i) + arrived(k))
        for b in range(4):
            for t in range(tiles):
                acc[t, pl.ds((4 * half + b) * nz, nz), :] = total[b, :, 128 * t : 128 * (t + 1)]

    for k in range(nz):
        for t in range(tiles):
            zsend[k, :, pl.ds(128 * t, 128)] = acc[t, pl.ds(k, n, stride=nz), :].astype(BF16)
    z_copy = []
    for k in range(1, nz):
        other = lax.rem(z + k, nz)
        z_copy.append(send(zsend.at[other], zrecv.at[z], zs.at[k], zr.at[k], {"fs_0": other}))
    zrecv[z] = zsend[z]

    for copy in r1_copy:
        copy.wait_recv()
    piece = rz[0]
    for s in range(1, nz):
        piece = piece + rz[s]
    ry[y] = piece
    r2_copy = [
        send(ry.at[y], ry.at[y], r2s.at[k], r2r.at[k], {"fs_1": lax.rem(y + k, ny)})
        for k in range(1, ny)
    ]

    for copy in c_copy[1:]:
        copy.wait_recv()
    cotc[j] = cotx[pl.ds(0, rows), pl.ds(pl.multiple_of(j * width, width), width)]
    mixed_all = jnp.concatenate([agb[s, pl.ds(2 * hidden, hidden), :] for s in range(n)], axis=1)
    gwd = dot_nn(mixed_all, cotc[...].reshape(n * rows, width))
    o_gwd[...] = gwd
    sq = gwd * gwd
    lanes = sq[:, 0:128]
    for k in range(1, tiles):
        lanes = lanes + sq[:, 128 * k : 128 * (k + 1)]
    drecv[j] = jnp.sum(lanes.T, axis=0, keepdims=True)
    d_copy = [
        send(drecv.at[j], drecv.at[j], ds_.at[k], dr.at[k], tp_device(k)) for k in range(1, n)
    ]

    for copy in r2_copy:
        copy.wait_recv()
    piece = ry[0]
    for s in range(1, ny):
        piece = piece + ry[s]
    for k in range(tiles):
        o_ra[:, pl.ds(128 * k, 128)] = piece[k]
        o_rv[:, pl.ds(128 * k, 128)] = piece[tiles + k]
    o_cr[...] = piece[2 * tiles]
    for copy in d_copy:
        copy.wait_recv()
    down = drecv[0]
    for s in range(1, n):
        down = down + drecv[s]
    o_rd[...] = down

    for copy in z_copy:
        copy.wait_recv()
    total = zrecv[0].astype(F32)
    for s in range(1, nz):
        total = total + zrecv[s].astype(F32)
    for a in range(n):
        row_out[slots[a]] = total[a : a + 1]
    for s in range(n):
        o_gi[:, pl.ds(width * s, width)] = row_out[s].astype(BF16)
    for copy in pend:
        copy.wait_send()


def finish(gi, gwa, gwv, gwd, tap, ra, rv, rd, cr,
           o_gi, o_gwa, o_gwv, o_gwd, o_gca, o_gcv, o_gba, o_gbv, o_ra, o_rv, o_rd, o_cr,
           csem):
    copies = [
        pltpu.make_async_copy(src, dst, csem.at[i])
        for i, (src, dst) in enumerate(((gwa, o_gwa), (gwv, o_gwv), (gwd, o_gwd)))
    ]
    for copy in copies:
        copy.start()
    o_gi[...] = gi[...]
    taps = tap[...]
    o_gca[...] = taps[0:3]
    o_gba[...] = taps[3:4]
    o_gcv[...] = taps[4:7]
    o_gbv[...] = taps[7:8]
    o_ra[...] = ra[...]
    o_rv[...] = rv[...]
    o_rd[...] = rd[...]
    o_cr[...] = jnp.concatenate([cr[:, 0:3], cr[:, 4:7]], axis=0)
    for copy in copies:
        copy.wait()


def per_device(sizes, hid, upa, upv, cot, wa, wv, wd, ca, cv, ba, bv):
    nz, ny, nx, nc = sizes
    n = nx * nc
    rows, hidden = upa.shape
    width = wd.shape[1]
    tokens = hid.shape[0]
    vm = pl.BlockSpec(memory_space=pltpu.VMEM)
    hbm = pl.BlockSpec(memory_space=pltpu.HBM)
    dma = pltpu.SemaphoreType.DMA

    def f32(*shape):
        return jax.ShapeDtypeStruct(shape, F32)

    outs = (
        jax.ShapeDtypeStruct((1, n * width), BF16),
        f32(hidden, width), f32(hidden, width), f32(hidden, width),
        f32(8, hidden), f32(1, width), f32(1, width), f32(1, hidden), f32(1, 128),
    )
    v = pltpu.VMEM
    scratch = [
        v((rows + 8, n * width), BF16), v((tokens, width), BF16), v((n, hidden, width), BF16),
        v((n, 2 * hidden, width), BF16), v((hidden, rows), BF16), v((hidden, rows), BF16),
        v(ca.shape, BF16), v(cv.shape, BF16), v(ba.shape, BF16), v(bv.shape, BF16),
        v((hidden, rows), BF16), v((hidden, rows), BF16), v((hidden, rows), BF16),
        v((n, 3 * hidden, rows), BF16), v((n, 8, hidden), F32), v((n, rows, width), BF16),
        v((rows, width), BF16), v((n, rows, width), F32),
        v((14, 4, nz, width), BF16), v((14, 4, nz, width), BF16),
        v((width // 128, rows, 128), F32), v((nz, n, width), BF16), v((nz, n, width), BF16),
        v((n, 1, width), F32),
        v((nz, 9, 1, 128), F32), v((ny, 9, 1, 128), F32), v((n, 1, hidden), F32),
        dma((11,)), dma((3,)), dma((3,)), dma((9,)), dma((9,)), dma((9,)), dma((9,)),
        dma((9,)), dma((9,)), dma((9,)), dma((9,)), dma((n,)), dma((n,)), dma((8,)), dma((8,)),
        dma((14,)), dma((14,)), dma((nz,)), dma((nz,)),
        dma((nz,)), dma((nz,)), dma((ny,)), dma((ny,)), dma((n,)), dma((n,)),
    ]
    res = pl.pallas_call(
        functools.partial(kernel, sizes),
        out_shape=outs,
        in_specs=[hbm] * 11,
        out_specs=[vm] * len(outs),
        scratch_shapes=scratch,
        compiler_params=pltpu.CompilerParams(
            collective_id=0, has_side_effects=True, vmem_limit_bytes=48 * 1024 * 1024
        ),
    )(*[pltpu.with_memory_space_constraint(v, pltpu.HBM) for v in (hid, upa.T, upv.T, cot, wa.T, wv.T, wd, ca, cv, ba, bv)])
    final = (
        jax.ShapeDtypeStruct((1, n * width), BF16),
        f32(hidden, width), f32(hidden, width), f32(hidden, width),
        f32(3, hidden), f32(3, hidden), f32(1, hidden), f32(1, hidden),
        f32(1, width), f32(1, width), f32(1, hidden), f32(2, 3),
    )
    gi, gwa, gwv, gwd, gca, gcv, gba, gbv, ra, rv, rd, conv_rows = pl.pallas_call(
        finish,
        out_shape=final,
        in_specs=[vm] * len(outs),
        out_specs=[vm, hbm, hbm, hbm] + [vm] * 8,
        scratch_shapes=[dma((3,))],
        compiler_params=pltpu.CompilerParams(vmem_limit_bytes=8 * 1024 * 1024),
    )(*res)
    return (
        gi, gwa.T, gwv.T, gwd, gca, gcv, gba[0], gbv[0], ra[0], rv[0], rd[0], conv_rows,
    )


def solution(mesh):
    sizes = (16, 8, 4, 2)
    finer = Mesh(mesh.devices.reshape(sizes), FS + TP)
    return jax.shard_map(
        functools.partial(per_device, sizes),
        mesh=finer,
        in_specs=(
            P(None, TP), P(TP, FS), P(TP, FS), P(TP, None), P(TP, FS), P(TP, FS),
            P(FS, TP), P(None, FS), P(None, FS), P(FS), P(FS),
        ),
        out_specs=(
            P(TP_FS, None), P(TP, FS), P(TP, FS), P(FS, TP), P(None, FS), P(None, FS),
            P(FS), P(FS), P(TP), P(TP), P(FS), P(),
        ),
        check_vma=False,
    )
```

time: 84.7 us -> 66.9 us (0.79)
  the two profiles are of different devices: /device:TPU:1 before, /device:TPU:6 now
where the time goes in v2:
time: 66.9 us; the launch traced here: 66.5 us
  Pallas kernels  65.8 us (98%)
    pallas_call x1, Pallas kernels, per_device(): pl.pallas_call(functools.partial(kernel, sizes), out_shape=outs, in_specs...  64.4 us
    pallas_call x1, Pallas kernels, per_device(): pl.pallas_call(finish, out_shape=final, in_specs=[vm] * len(outs), out_sp...  1.47 us

profile of v2, /device:TPU:6, one launch (start us, length us, event | category | flops | bytes accessed | tf_op | source)
XLA Modules:
  0.0 66.5 jit_solution(9355244801265132056)
XLA Ops:
  0.6 64.4 %shard_map.202 = (bf16[1,4096]{1,0:T(2,128)(2,1)S(1)}, f32[96,512]{1,0:T(8,128)S(1)}, f32[96,512]{1,0:T(8,128)S(1)}, f32[96,512]{1,0:T(8,128)S(1)}, f32[8,96]{1,...) custom-call(bf16[1024,512]{1,0:T(8,128)(2,1)} %hid.1, ...), custom_call_target="tpu_custom_call" | custom-call | tf_op jit(solution)/shard_map/pallas_call | solution.py:476
  65.0 1.5 %shard_map.203 = (bf16[1,4096]{1,0:T(2,128)(2,1)}, f32[96,512]{1,0:T(8,128)}, f32[96,512]{1,0:T(8,128)}, f32[96,512]{1,0:T(8,128)}, f32[3,96]{1,0:T(4,128)}, /*i...) custom-call(bf16[1,4096]{1,0:T(2,128)(2,1)S(1)} %get-tuple-element.3, ...), custom_call_target="tpu_custom_call" | custom-call | tf_op jit(solution)/shard_map/pallas_call | solution.py:492

commit v3 on v2

--- a/solution.py
+++ b/solution.py
@@ -34,7 +34,7 @@
     agb, tapb, cotc, relay, pbuf, ysend, yrecv, acc, zsend, zrecv, row_out,
     rz, ry, drecv,
     lsem, hs, hr, wds_, wdr, was, war, wvs, wvr, gs, gr, ts, tr, cs, cr,
-    ys, yr, zs, zr, r1s, r1r, r2s, r2r, ds_, dr,
+    ys, yr, zs, zr, r1s, r1r, r2s, r2r, ds_, dr, tok,
 ):
     nz, ny, nx, nc = sizes
     z, y = lax.axis_index("fs_0"), lax.axis_index("fs_1")
@@ -60,10 +60,14 @@
         other = lax.rem(j + k, n)
         return {"tp_0": other // nc, "tp_1": lax.rem(other, nc)}
 
-    for k in range(1, nz):
-        pl.semaphore_signal(barrier, inc=1, device_id={"fs_0": lax.rem(z + k, nz)}, device_id_type=MESH)
-    for k in range(1, ny):
-        pl.semaphore_signal(barrier, inc=1, device_id={"fs_1": lax.rem(y + k, ny)}, device_id_type=MESH)
+    def both_sides(sem, axis, at, length, by):
+        for k in (by, length - by):
+            pl.semaphore_signal(
+                sem, inc=1, device_id={axis: lax.rem(at + k, length)}, device_id_type=MESH
+            )
+
+    both_sides(barrier, "fs_0", z, nz, 1)
+    both_sides(barrier, "fs_1", y, ny, 1)
     for k in range(1, n):
         pl.semaphore_signal(barrier, inc=1, device_id=tp_device(k), device_id_type=MESH)
 
@@ -89,7 +93,10 @@
     tails = jnp.where(lane >= rows - 2, ua, roll(uv, -2))
     hb[...] = jnp.where(lane < rows // 2, heads, tails).astype(BF16)
 
-    pl.semaphore_wait(barrier, n - 1 + ny - 1 + nz - 1)
+    pl.semaphore_wait(barrier, n - 1 + 4)
+
+    both_sides(tok.at[0], "fs_0", z, nz, 1)
+    both_sides(tok.at[1], "fs_1", y, ny, 1)
 
     partner = {"tp_1": 1 - c}
 
@@ -114,8 +121,11 @@
             self.copies[i] = send(view, view, self.ssem.at[i], self.rsem.at[i], device)
 
         def start(self):
-            self.go(1, j, 0, self.count, chip(1))
-            self.go(2, j, 0, self.count, chip(3))
+            half = self.half
+            self.go(1, j, 0, half, chip(1))
+            self.go(2, j, half, half, chip(3))
+            self.go(9, j, half, half, chip(1))
+            self.go(10, j, 0, half, chip(3))
             self.go(0, j, 0, self.count, partner)
 
         def wait(self, *which):
@@ -125,9 +135,11 @@
         def pass_near(self):
             self.wait(1)
             self.go(3, slots[2], 0, self.half, chip(1))
-            self.go(5, slots[2], 0, self.count, partner)
             self.wait(2)
             self.go(4, slots[3], self.half, self.half, chip(3))
+            self.wait(9)
+            self.go(5, slots[2], 0, self.count, partner)
+            self.wait(10)
             self.go(6, slots[3], 0, self.count, partner)
 
         def pass_far(self):
@@ -162,6 +174,12 @@
     par_a = [table[:, k : k + 1] for k in range(4)]
     par_v = [table[:, k : k + 1] for k in range(4, 8)]
 
+    down_all.pass_near()
+    val_all.start()
+    pl.semaphore_wait(tok.at[0], 2)
+    pl.semaphore_wait(tok.at[1], 2)
+    both_sides(tok.at[2], "fs_0", z, nz, 2)
+    both_sides(tok.at[3], "fs_1", y, ny, 2)
     for copy in h_copy:
         copy.wait_recv()
     first = (j > 0).astype(F32)
@@ -205,14 +223,15 @@
     gm = part(j, wdall[j])
     down_all.wait(0)
     gm = gm + part(slots[1], wdall[slots[1]])
-    down_all.pass_near()
-    val_all.start()
     gm = gm + part(slots[2], wdall[slots[2]]) + part(slots[3], wdall[slots[3]])
     down_all.wait(5, 6)
     gm = gm + part(slots[4], wdall[slots[4]]) + part(slots[5], wdall[slots[5]])
     act_all.pass_near()
     down_all.pass_far()
     gm = gm + part(slots[6], wdall[slots[6]])
+    pl.semaphore_wait(tok.at[2], 2)
+    pl.semaphore_wait(tok.at[3], 2)
+    both_sides(tok.at[4], "fs_0", z, nz, 4)
     down_all.wait(7, 8)
     gm = gm + part(slots[7], wdall[slots[7]])
     gm = gm.astype(BF16).astype(F32)
@@ -231,20 +250,7 @@
     agb[j, pl.ds(0, hidden), :] = behind(par_a, grad_a, after_a).astype(BF16)
     agb[j, pl.ds(hidden, hidden), :] = behind(par_v, grad_v, after_v).astype(BF16)
     val_all.pass_near()
-    grads_all.start()
     left = dot_nt(order, agb[j, pl.ds(0, 2 * hidden), :]).astype(BF16)
-
-    spread = jnp.zeros((hidden, rows), F32)
-    at = 0
-    for grad, ups in ((grad_a, ups_a), (grad_v, ups_v)):
-        for k in range(4):
-            terms = grad * ups[k] if k < 3 else grad
-            spread = jnp.where(lane == at, jnp.sum(terms, axis=1, keepdims=True), spread)
-            at += 1
-    tapb[j] = spread.T[0:8]
-    t_copy = [
-        send(tapb.at[j], tapb.at[j], ts.at[k], tr.at[k], tp_device(k)) for k in range(1, n)
-    ]
 
     def product(a):
         pbuf[a] = dot_nn(left, wall[slots[a]])
@@ -273,6 +279,8 @@
     product(3)
     pass_on(0, mine(4, 0), 1)
     pass_on(11, mine(-3, 0), -1)
+    grads_all.start()
+
     act_all.wait(5, 6)
     val_all.wait(5, 6)
     product(4)
@@ -285,6 +293,18 @@
     product(7)
     pass_on(7, mine(-4, 1), -1)
     pass_on(4, mine(3, 1), 1)
+    spread = jnp.zeros((hidden, rows), F32)
+    at = 0
+    for grad, ups in ((grad_a, ups_a), (grad_v, ups_v)):
+        for k in range(4):
+            terms = grad * ups[k] if k < 3 else grad
+            spread = jnp.where(lane == at, jnp.sum(terms, axis=1, keepdims=True), spread)
+            at += 1
+    tapb[j] = spread.T[0:8]
+    t_copy = [
+        send(tapb.at[j], tapb.at[j], ts.at[k], tr.at[k], tp_device(k)) for k in range(1, n)
+    ]
+
     grads_all.pass_near()
     pass_on(1, arrived(0) + mine(3, 0), 1)
     pass_on(12, arrived(11) + mine(-2, 0), -1)
@@ -333,6 +353,7 @@
     for k in range(tiles):
         rz[z, k] = row_a[:, 128 * k : 128 * (k + 1)]
         rz[z, tiles + k] = row_v[:, 128 * k : 128 * (k + 1)]
+    pl.semaphore_wait(tok.at[4], 2)
     rz[z, 2 * tiles] = jnp.sum(jnp.where(spot, sums, 0.0), axis=0, keepdims=True)
     r1_copy = [
         send(rz.at[z], rz.at[z], r1s.at[k], r1r.at[k], {"fs_0": lax.rem(z + k, nz)})
@@ -345,20 +366,26 @@
     c_copy[0].wait_recv()
     c_copy.append(send(relay, cotc.at[slot_of(3, 1 - c)], cs.at[7], cr.at[7], chip(3)))
     pass_on(10, arrived(9) + mine(-1, 1), -1)
+    z_copy = []
     for half, (i, k) in enumerate(((13, 3), (6, 10))):
         total = mine(0, half) + (arrived(i) + arrived(k))
         for b in range(4):
             for t in range(tiles):
-                acc[t, pl.ds((4 * half + b) * nz, nz), :] = total[b, :, 128 * t : 128 * (t + 1)]
-
-    for k in range(nz):
-        for t in range(tiles):
-            zsend[k, :, pl.ds(128 * t, 128)] = acc[t, pl.ds(k, n, stride=nz), :].astype(BF16)
-    z_copy = []
-    for k in range(1, nz):
-        other = lax.rem(z + k, nz)
-        z_copy.append(send(zsend.at[other], zrecv.at[z], zs.at[k], zr.at[k], {"fs_0": other}))
-    zrecv[z] = zsend[z]
+                acc[half, t, pl.ds(b * nz, nz), :] = total[b, :, 128 * t : 128 * (t + 1)]
+        for k in range(nz):
+            for t in range(tiles):
+                zsend[half, k, :, pl.ds(128 * t, 128)] = acc[
+                    half, t, pl.ds(k, 4, stride=nz), :
+                ].astype(BF16)
+        for k in range(1, nz):
+            other = lax.rem(z + k, nz)
+            z_copy.append(
+                send(
+                    zsend.at[half, other], zrecv.at[half, z], zs.at[half, k], zr.at[half, k],
+                    {"fs_0": other},
+                )
+            )
+        zrecv[half, z] = zsend[half, z]
 
     for copy in r1_copy:
         copy.wait_recv()
@@ -404,11 +431,12 @@
 
     for copy in z_copy:
         copy.wait_recv()
-    total = zrecv[0].astype(F32)
-    for s in range(1, nz):
-        total = total + zrecv[s].astype(F32)
-    for a in range(n):
-        row_out[slots[a]] = total[a : a + 1]
+    for half in range(2):
+        total = zrecv[half, 0].astype(F32)
+        for s in range(1, nz):
+            total = total + zrecv[half, s].astype(F32)
+        for a in range(4):
+            row_out[slots[4 * half + a]] = total[a : a + 1]
     for s in range(n):
         o_gi[:, pl.ds(width * s, width)] = row_out[s].astype(BF16)
     for copy in pend:
@@ -465,13 +493,15 @@
         v((n, 3 * hidden, rows), BF16), v((n, 8, hidden), F32), v((n, rows, width), BF16),
         v((rows, width), BF16), v((n, rows, width), F32),
         v((14, 4, nz, width), BF16), v((14, 4, nz, width), BF16),
-        v((width // 128, rows, 128), F32), v((nz, n, width), BF16), v((nz, n, width), BF16),
+        v((2, width // 128, 4 * nz, 128), F32),
+        v((2, nz, 4, width), BF16), v((2, nz, 4, width), BF16),
         v((n, 1, width), F32),
         v((nz, 9, 1, 128), F32), v((ny, 9, 1, 128), F32), v((n, 1, hidden), F32),
-        dma((11,)), dma((3,)), dma((3,)), dma((9,)), dma((9,)), dma((9,)), dma((9,)),
-        dma((9,)), dma((9,)), dma((9,)), dma((9,)), dma((n,)), dma((n,)), dma((8,)), dma((8,)),
-        dma((14,)), dma((14,)), dma((nz,)), dma((nz,)),
+        dma((11,)), dma((3,)), dma((3,)), dma((11,)), dma((11,)), dma((11,)), dma((11,)),
+        dma((11,)), dma((11,)), dma((11,)), dma((11,)), dma((n,)), dma((n,)), dma((8,)), dma((8,)),
+        dma((14,)), dma((14,)), dma((2, nz)), dma((2, nz)),
         dma((nz,)), dma((nz,)), dma((ny,)), dma((ny,)), dma((n,)), dma((n,)),
+        pltpu.SemaphoreType.REGULAR((5,)),
     ]
     res = pl.pallas_call(
         functools.partial(kernel, sizes),

time: 66.9 us -> 61.9 us (0.925)
  Pallas kernels: 65.8 us -> 60.4 us
    pallas_call x1, Pallas kernels: 64.4 us -> 58.9 us  [per_device(): pl.pallas_call(functools.partial(kernel, sizes), out_shape=outs, in_specs...]
where the time goes in v3:
time: 61.9 us; the launch traced here: 61 us
  Pallas kernels  60.4 us (98%)
  between operations  0.66 us (1%)
    pallas_call x1, Pallas kernels, per_device(): pl.pallas_call(functools.partial(kernel, sizes), out_shape=outs, in_specs...  58.9 us
    pallas_call x1, Pallas kernels, per_device(): pl.pallas_call(finish, out_shape=final, in_specs=[vm] * len(outs), out_sp...  1.47 us

profile of v3, /device:TPU:6, one launch (start us, length us, event | category | flops | bytes accessed | tf_op | source)
XLA Modules:
  0.0 61.0 jit_solution(12966305258274460608)
XLA Ops:
  0.6 58.9 %shard_map.202 = (bf16[1,4096]{1,0:T(2,128)(2,1)S(1)}, f32[96,512]{1,0:T(8,128)S(1)}, f32[96,512]{1,0:T(8,128)S(1)}, f32[96,512]{1,0:T(8,128)S(1)}, f32[8,96]{1,...) custom-call(bf16[1024,512]{1,0:T(8,128)(2,1)} %hid.1, ...), custom_call_target="tpu_custom_call" | custom-call | tf_op jit(solution)/shard_map/pallas_call | solution.py:506
  59.5 1.5 %shard_map.203 = (bf16[1,4096]{1,0:T(2,128)(2,1)}, f32[96,512]{1,0:T(8,128)}, f32[96,512]{1,0:T(8,128)}, f32[96,512]{1,0:T(8,128)}, f32[3,96]{1,0:T(4,128)}, /*i...) custom-call(bf16[1,4096]{1,0:T(2,128)(2,1)S(1)} %get-tuple-element.3, ...), custom_call_target="tpu_custom_call" | custom-call | tf_op jit(solution)/shard_map/pallas_call | solution.py:522

commit v4 on v3

--- a/solution.py
+++ b/solution.py
@@ -429,9 +429,11 @@
         down = down + drecv[s]
     o_rd[...] = down
 
-    for copy in z_copy:
-        copy.wait_recv()
+    for copy in pend:
+        copy.wait_send()
     for half in range(2):
+        for copy in z_copy[half * (nz - 1) : (half + 1) * (nz - 1)]:
+            copy.wait_recv()
         total = zrecv[half, 0].astype(F32)
         for s in range(1, nz):
             total = total + zrecv[half, s].astype(F32)
@@ -439,29 +441,26 @@
             row_out[slots[4 * half + a]] = total[a : a + 1]
     for s in range(n):
         o_gi[:, pl.ds(width * s, width)] = row_out[s].astype(BF16)
-    for copy in pend:
-        copy.wait_send()
 
 
 def finish(gi, gwa, gwv, gwd, tap, ra, rv, rd, cr,
            o_gi, o_gwa, o_gwv, o_gwd, o_gca, o_gcv, o_gba, o_gbv, o_ra, o_rv, o_rd, o_cr,
-           csem):
+           t_gca, t_gcv, t_gba, t_gbv, t_cr, csem):
+    taps = tap[...]
+    t_gca[...] = taps[0:3]
+    t_gba[...] = taps[3:4]
+    t_gcv[...] = taps[4:7]
+    t_gbv[...] = taps[7:8]
+    t_cr[...] = jnp.concatenate([cr[:, 0:3], cr[:, 4:7]], axis=0)
     copies = [
         pltpu.make_async_copy(src, dst, csem.at[i])
-        for i, (src, dst) in enumerate(((gwa, o_gwa), (gwv, o_gwv), (gwd, o_gwd)))
+        for i, (src, dst) in enumerate((
+            (gwa, o_gwa), (gwv, o_gwv), (gwd, o_gwd), (gi, o_gi), (ra, o_ra), (rv, o_rv), (rd, o_rd),
+            (t_gca, o_gca), (t_gcv, o_gcv), (t_gba, o_gba), (t_gbv, o_gbv), (t_cr, o_cr),
+        ))
     ]
     for copy in copies:
         copy.start()
-    o_gi[...] = gi[...]
-    taps = tap[...]
-    o_gca[...] = taps[0:3]
-    o_gba[...] = taps[3:4]
-    o_gcv[...] = taps[4:7]
-    o_gbv[...] = taps[7:8]
-    o_ra[...] = ra[...]
-    o_rv[...] = rv[...]
-    o_rd[...] = rd[...]
-    o_cr[...] = jnp.concatenate([cr[:, 0:3], cr[:, 4:7]], axis=0)
     for copy in copies:
         copy.wait()
 
@@ -523,8 +522,8 @@
         finish,
         out_shape=final,
         in_specs=[vm] * len(outs),
-        out_specs=[vm, hbm, hbm, hbm] + [vm] * 8,
-        scratch_shapes=[dma((3,))],
+        out_specs=[hbm] * 12,
+        scratch_shapes=[v(o.shape, F32) for o in (final[4], final[5], final[6], final[7], final[11])] + [dma((12,))],
         compiler_params=pltpu.CompilerParams(vmem_limit_bytes=8 * 1024 * 1024),
     )(*res)
     return (

time: 61.9 us -> 61.2 us (0.989)
  Pallas kernels: 60.4 us -> 59.6 us
where the time goes in v4:
time: 61.2 us; the launch traced here: 60.3 us
  Pallas kernels  59.6 us (97%)
  between operations  0.66 us (1%)
    pallas_call x1, Pallas kernels, per_device(): pl.pallas_call(functools.partial(kernel, sizes), out_shape=outs, in_specs...  58.7 us

profile of v4, /device:TPU:6, one launch (start us, length us, event | category | flops | bytes accessed | tf_op | source)
XLA Modules:
  0.0 60.3 jit_solution(16675450777730838812)
XLA Ops:
  0.6 58.7 %shard_map.202 = (bf16[1,4096]{1,0:T(2,128)(2,1)S(1)}, f32[96,512]{1,0:T(8,128)S(1)}, f32[96,512]{1,0:T(8,128)S(1)}, f32[96,512]{1,0:T(8,128)S(1)}, f32[8,96]{1,...) custom-call(bf16[1024,512]{1,0:T(8,128)(2,1)} %hid.1, ...), custom_call_target="tpu_custom_call" | custom-call | tf_op jit(solution)/shard_map/pallas_call | solution.py:505
  59.3 0.9 %shard_map.203 = (bf16[1,4096]{1,0:T(2,128)(2,1)}, f32[96,512]{1,0:T(8,128)}, f32[96,512]{1,0:T(8,128)}, f32[96,512]{1,0:T(8,128)}, f32[3,96]{1,0:T(4,128)}, /*i...) custom-call(bf16[1,4096]{1,0:T(2,128)(2,1)S(1)} %get-tuple-element.3, ...), custom_call_target="tpu_custom_call" | custom-call | tf_op jit(solution)/shard_map/pallas_call | solution.py:521
